TPU v7x, 32 devices: a whole 2x2x4 slice. The times are simulated.
32 devices in a mesh: grp: 2 (over y), kv: 4 (over z), tp: 4 (over x, core).
Axes of the slice: x: 2, y: 2, z: 4, core: 2. Of those that a mesh axis runs over, the one named last changes fastest.
Arguments:
- tokens: bfloat16 [64, 4096], P('grp', ('kv', 'tp')), parts along dimension 0, may hold values from -8 to 8
- norm_gain: bfloat16 [4096], P('kv'), may hold values from 0.099609375 to 1.8984375
- w_query: bfloat16 [4096, 1024], P('kv', 'tp'), may hold values from -0.09375 to 0.09375
- w_key: bfloat16 [4096, 1024], P('kv', 'tp'), may hold values from -0.09375 to 0.09375
- w_value: bfloat16 [4096, 2048], P('kv', 'tp'), may hold values from -0.09375 to 0.09375
- w_ogate: bfloat16 [4096, 2048], P('kv', 'tp'), may hold values from -0.09375 to 0.09375
- w_igate: bfloat16 [4096, 16], P('kv', 'tp'), may hold values from -0.09375 to 0.09375
- w_fgate: bfloat16 [4096, 16], P('kv', 'tp'), may hold values from -0.09375 to 0.09375
- igate_bias: float32 [16], P('tp'), may hold values from -1 to 1
- fgate_bias: float32 [16], P('tp'), may hold values from -1 to 4
- state_c: float32 [64, 16, 64, 128], P(('grp', 'kv'), 'tp'), parts along dimension 0, may hold values from -1.5 to 1.5
- state_n: float32 [64, 16, 64], P(('grp', 'kv'), 'tp'), parts along dimension 0, may hold values from -1.5 to 1.5
- state_m: float32 [64, 16], P(('grp', 'kv'), 'tp'), parts along dimension 0, may hold values from -3 to 1
- head_gain: bfloat16 [16, 128], P('tp'), may hold values from 0.099609375 to 1.8984375
- w_out: bfloat16 [2048, 4096], P('tp', 'kv'), may hold values from -0.125 to 0.125
- ffn_gain: bfloat16 [4096], P('kv'), may hold values from 0.099609375 to 1.8984375
- w_gate: bfloat16 [4096, 11008], P('kv', 'tp'), may hold values from -0.09375 to 0.09375
- w_up: bfloat16 [4096, 11008], P('kv', 'tp'), may hold values from -0.09375 to 0.09375
- w_down: bfloat16 [11008, 4096], P('tp', 'kv'), may hold values from -0.0546875 to 0.0546875
Outputs:
- out_tokens: bfloat16 [64, 4096], P('grp', ('kv', 'tp')), parts along dimension 0
- new_c: float32 [64, 16, 64, 128], P(('grp', 'kv'), 'tp'), parts along dimension 0
- new_n: float32 [64, 16, 64], P(('grp', 'kv'), 'tp'), parts along dimension 0
- new_m: float32 [64, 16], P(('grp', 'kv'), 'tp'), parts along dimension 0
There are 2 independent parts, one for each index of `grp`. A program takes and returns all parts, laid end to end along the dimension named above; an argument that names none is the same for every part. Nothing has to cross between parts.
All inputs are finite; a program needn't handle non-finite values.
Results may differ from a plain program's by a relative error of at most 0.017.
Values may be sent and summed in bfloat16 or wider, within the bound.
A program may use at most 64 MiB of HBM per device.

v0:
```python
import jax
import jax.numpy as jnp
from jax import lax
from jax.sharding import PartitionSpec as P

D = 4096
DK = 64
DV = 128


norm_eps = 1e-06
igate_cap = 1.5


def cell_update(query, key_vec, value_vec, igate, fgate, state_c, state_n, state_m):
    carried = jax.nn.log_sigmoid(fgate) + state_m
    new_m = jnp.maximum(carried, igate)
    keep_weight = jnp.exp(carried - new_m)
    write_weight = jnp.exp(igate - new_m)
    new_c = (
        keep_weight[..., None, None] * state_c
        + write_weight[..., None, None] * key_vec[..., :, None] * value_vec[..., None, :]
    )
    new_n = keep_weight[..., None] * state_n + write_weight[..., None] * key_vec
    numerator = jnp.einsum("bhd,bhde->bhe", query, new_c, precision=lax.Precision.HIGHEST)
    denominator = jnp.sum(query * new_n, axis=-1)
    head_out = numerator / jnp.maximum(jnp.abs(denominator), jnp.exp(-new_m))[..., None]
    return (new_c, new_n, new_m, head_out)


def body(
    tokens,
    norm_gain,
    w_query,
    w_key,
    w_value,
    w_ogate,
    w_igate,
    w_fgate,
    igate_bias,
    fgate_bias,
    state_c,
    state_n,
    state_m,
    head_gain,
    w_out,
    ffn_gain,
    w_gate,
    w_up,
    w_down,
):
    seq_rows = state_c.shape[0]
    heads_here = state_c.shape[1]
    token_cols = lax.all_gather(tokens, "tp", axis=1, tiled=True)
    token_vals = token_cols.astype(jnp.float32)
    normed = (token_vals * norm_gain.astype(jnp.float32)).astype(jnp.bfloat16)
    squares = jnp.sum(token_vals * token_vals, axis=1)
    part_query = jnp.dot(normed, w_query, preferred_element_type=jnp.float32)
    part_key = jnp.dot(normed, w_key, preferred_element_type=jnp.float32)
    part_value = jnp.dot(normed, w_value, preferred_element_type=jnp.float32)
    part_ogate = jnp.dot(normed, w_ogate, preferred_element_type=jnp.float32)
    part_igate = jnp.dot(normed, w_igate, preferred_element_type=jnp.float32)
    part_fgate = jnp.dot(normed, w_fgate, preferred_element_type=jnp.float32)
    all_squares = lax.psum(squares, "kv")
    sum_squares = lax.dynamic_slice_in_dim(
        all_squares, lax.axis_index("kv") * seq_rows, seq_rows, 0
    )
    sum_query, sum_key, sum_value, sum_ogate, sum_igate, sum_fgate = (
        lax.psum_scatter(part_query, "kv", scatter_dimension=0, tiled=True),
        lax.psum_scatter(part_key, "kv", scatter_dimension=0, tiled=True),
        lax.psum_scatter(part_value, "kv", scatter_dimension=0, tiled=True),
        lax.psum_scatter(part_ogate, "kv", scatter_dimension=0, tiled=True),
        lax.psum_scatter(part_igate, "kv", scatter_dimension=0, tiled=True),
        lax.psum_scatter(part_fgate, "kv", scatter_dimension=0, tiled=True),
    )
    row_scale = lax.rsqrt(sum_squares / D + norm_eps)[:, None]
    query = (row_scale * sum_query).reshape(seq_rows, heads_here, DK)
    key_vec = (row_scale * sum_key).reshape(seq_rows, heads_here, DK) * DK ** (-0.5)
    value_vec = (row_scale * sum_value).reshape(seq_rows, heads_here, DV)
    ogate = (row_scale * sum_ogate).reshape(seq_rows, heads_here, DV)
    igate = igate_cap * jnp.tanh((row_scale * sum_igate + igate_bias) / igate_cap)
    fgate = row_scale * sum_fgate + fgate_bias
    new_c, new_n, new_m, head_out = cell_update(
        query, key_vec, value_vec, igate, fgate, state_c, state_n, state_m
    )
    merged = (
        (head_out * head_gain.astype(jnp.float32) * jax.nn.sigmoid(ogate))
        .reshape(seq_rows, heads_here * DV)
        .astype(jnp.bfloat16)
    )
    attn_part = jnp.dot(
        lax.all_gather(merged, "kv", axis=0, tiled=True), w_out, preferred_element_type=jnp.float32
    )
    attn_out = lax.psum_scatter(
        attn_part.astype(jnp.bfloat16), "tp", scatter_dimension=1, tiled=True
    ).astype(jnp.float32)
    middle = (tokens.astype(jnp.float32) + attn_out).astype(jnp.bfloat16)
    middle_cols = lax.all_gather(middle, "tp", axis=1, tiled=True)
    middle_vals = middle_cols.astype(jnp.float32)
    normed_two = (middle_vals * ffn_gain.astype(jnp.float32)).astype(jnp.bfloat16)
    squares_two = jnp.sum(middle_vals * middle_vals, axis=1)
    gate_part = jnp.dot(normed_two, w_gate, preferred_element_type=jnp.float32)
    up_part = jnp.dot(normed_two, w_up, preferred_element_type=jnp.float32)
    gate_sum, up_sum, total_two = (
        lax.psum(gate_part.astype(jnp.bfloat16), "kv").astype(jnp.float32),
        lax.psum(up_part.astype(jnp.bfloat16), "kv").astype(jnp.float32),
        lax.psum(squares_two.astype(jnp.bfloat16), "kv").astype(jnp.float32),
    )
    ffn_scale = lax.rsqrt(total_two / D + norm_eps)[:, None]
    hidden = (jax.nn.silu(ffn_scale * gate_sum) * (ffn_scale * up_sum)).astype(jnp.bfloat16)
    down_part = jnp.dot(hidden, w_down, preferred_element_type=jnp.float32)
    down_out = lax.psum_scatter(
        down_part.astype(jnp.bfloat16), "tp", scatter_dimension=1, tiled=True
    ).astype(jnp.float32)
    out_tokens = (middle.astype(jnp.float32) + down_out).astype(jnp.bfloat16)
    return (out_tokens, new_c, new_n, new_m)


def solution(mesh):
    placed = (
        P("grp", ("kv", "tp")),
        P("kv"),
        P("kv", "tp"),
        P("kv", "tp"),
        P("kv", "tp"),
        P("kv", "tp"),
        P("kv", "tp"),
        P("kv", "tp"),
        P("tp"),
        P("tp"),
        P(("grp", "kv"), "tp", None, None),
        P(("grp", "kv"), "tp", None),
        P(("grp", "kv"), "tp"),
        P("tp", None),
        P("tp", "kv"),
        P("kv"),
        P("kv", "tp"),
        P("kv", "tp"),
        P("tp", "kv"),
    )
    return jax.shard_map(
        body,
        mesh=mesh,
        in_specs=placed,
        out_specs=(
            P("grp", ("kv", "tp")),
            P(("grp", "kv"), "tp", None, None),
            P(("grp", "kv"), "tp", None),
            P(("grp", "kv"), "tp"),
        ),
        check_vma=False,
    )
```

profile of v0, /device:TPU:0, one launch (start us, length us, event | category | flops | bytes accessed | tf_op | source)
XLA Modules:
  0.0 214.9 jit_solution(8268883809326724830)
XLA Ops:
  7.2 0.0 copy-start
  7.2 0.0 copy-start.2
  7.2 0.0 reduce-scatter.11.cloned.1.call-start
  7.2 0.8 convert_element_type.74
  8.0 6.4 %all_gather.9 = bf16[32,1024]{1,0:T(8,128)(2,1)S(1)} all-gather(bf16[32,256]{1,0:T(8,128)(2,1)} %param.19), channel_id=1, replica_groups=mesh['grp'=2,'kv'=4,'tp'=4] {'tp'}, dimensions={1}, use_global_device_ids=true | all-gather | bytes 81920 | tf_op jit(solution)/shard_map/all_gather | solution.py:54
  14.4 1.8 fusion.12
  16.3 0.0 reduce-scatter.11.cloned.1.call-update
  16.3 0.0 reduce-scatter.9.cloned.1.call-start
  16.4 1.8 fusion.18
  18.2 0.0 reduce-scatter.9.cloned.1.call-update
  18.2 0.0 reduce-scatter.13.cloned.1.call-start
  18.3 2.1 fusion.10
  20.4 0.0 reduce-scatter.13.cloned.1.call-update
  20.4 0.0 reduce-scatter.15.cloned.1.call-start
  20.5 2.1 fusion.8
  22.6 0.0 reduce-scatter.15.cloned.1.call-update
  22.6 0.0 reduce-scatter.17.cloned.1.call-start
  22.7 0.1 fusion.2
  22.8 0.7 convert_element_type.76
  23.5 0.8 copy.28
  24.3 0.8 fusion.16
  25.1 0.8 fusion.14
  25.9 1.2 dynamic-slice
  27.8 12.6 %all-reduce.2 = (f32[32]{0:T(128)S(1)}, f32[32,4]{0,1:T(4,128)S(1)}, f32[32,4]{0,1:T(4,128)S(1)}) all-reduce(f32[32]{0:T(128)S(1)} %fusion.2, f32[32,4]{0,1:T(4,128)S(1)} %fusion.14, f32[32,4]{0,1:T(4,128)S(1)} %fusion.16), channel_id=1, replica_groups=mesh['grp'=2,'kv'=4,'tp'=4] {'kv'}, use_global_device_ids=true, to_apply=%region_1.0 | all-reduce | flops 288 | bytes 2304 | tf_op jit(solution)/shard_map/psum | solution.py:64
  40.4 0.1 constant_dynamic-slice_fusion
  40.5 0.1 copy.29
  40.6 0.1 copy.27
  40.6 0.1 add_rsqrt_fusion.1
  40.7 0.8 subtract_exponential_fusion
  41.5 0.7 exponential_multiply_fusion
  42.2 14.9 %reduce-scatter.9.cloned.1.call-done = f32[8,256]{1,0:T(8,128)} async-done(((f32[32,256]{1,0:T(8,128)}), f32[8,256]{1,0:T(8,128)}) %reduce-scatter.9.cloned.1.call-update) | async-done | bytes 8208 | tf_op jit(solution)/shard_map/reduce_scatter | solution.py:69
  57.1 0.8 broadcast_multiply_fusion.1
  57.9 0.1 reshape.46
  58.0 0.1 reshape.44
  58.0 0.1 reshape.45
  58.1 1.4 multiply_reduce_fusion
  59.5 0.1 copy.31
  59.6 17.8 %reduce-scatter.13.cloned.1.call-done = f32[8,512]{1,0:T(8,128)} async-done(((f32[32,512]{1,0:T(8,128)}), f32[8,512]{1,0:T(8,128)}) %reduce-scatter.13.cloned.1.call-update) | async-done | bytes 16400 | tf_op jit(solution)/shard_map/reduce_scatter | solution.py:71
  77.4 0.8 multiply_bitcast_fusion
  78.2 1.6 multiply_add_fusion
  79.8 0.0 copy-start.1
  79.8 1.0 fusion.28
  80.8 16.2 %reduce-scatter.15.cloned.1.call-done = f32[8,512]{1,0:T(8,128)} async-done(((f32[32,512]{1,0:T(8,128)}), f32[8,512]{1,0:T(8,128)}) %reduce-scatter.15.cloned.1.call-update) | async-done | bytes 16400 | tf_op jit(solution)/shard_map/reduce_scatter | solution.py:72
  97.0 0.8 fusion.22
  97.8 13.1 %all_gather.10 = bf16[32,512]{1,0:T(8,128)(2,1)S(1)} all-gather(bf16[8,512]{1,0:T(8,128)(2,1)S(1)} %fusion.22), channel_id=1, replica_groups=mesh['grp'=2,'kv'=4,'tp'=4] {'kv'}, dimensions={0}, use_global_device_ids=true | all-gather | bytes 40960 | tf_op jit(solution)/shard_map/all_gather | solution.py:92
  110.9 0.9 convolution_convert_fusion.3
  111.8 0.0 reduce-scatter.17.cloned.1.call-update
  111.9 0.0 all-reduce.6.cloned.1.call-start
  111.9 17.8 %reduce-scatter.17.cloned.1.call-done = bf16[32,256]{1,0:T(8,128)(2,1)} async-done(((bf16[32,1024]{1,0:T(8,128)(2,1)}), bf16[32,256]{1,0:T(8,128)(2,1)}) %reduce-scatter.17.cloned.1.call-update) | async-done | bytes 16400 | tf_op jit(solution)/shard_map/reduce_scatter | solution.py:94
  129.8 0.0 copy-done.2
  129.8 0.7 add_convert_fusion.1
  130.5 5.2 %all_gather.11 = bf16[32,1024]{1,0:T(8,128)(2,1)S(1)} all-gather(bf16[32,256]{1,0:T(8,128)(2,1)S(1)} %add_convert_fusion.1), channel_id=1, replica_groups=mesh['grp'=2,'kv'=4,'tp'=4] {'tp'}, dimensions={1}, use_global_device_ids=true | all-gather | bytes 81920 | tf_op jit(solution)/shard_map/all_gather | solution.py:98
  135.7 5.0 %convolution_convert_fusion = bf16[32,2752]{1,0:T(8,128)(2,1)} fusion(bf16[1024,2752]{0,1:T(8,128)(2,1)} %param.36, bf16[32,1024]{1,0:T(8,128)(2,1)S(1)} %all_gather.11, f32[1024]{0:T(1024)S(1)} %convert_element_type.86), kind=kOutput, calls=%fused_computation | convolution fusion | flops 180541440 | bytes 5881856 | tf_op jit(solution)/shard_map/dot_general | solution.py:103
  140.8 5.0 %convolution_convert_fusion.1 = bf16[32,2752]{1,0:T(8,128)(2,1)} fusion(bf16[1024,2752]{0,1:T(8,128)(2,1)} %param.35, bf16[32,1024]{1,0:T(8,128)(2,1)S(1)} %all_gather.11, f32[1024]{0:T(1024)S(1)} %convert_element_type.86), kind=kOutput, calls=%fused_computation.1 | convolution fusion | flops 180541440 | bytes 5881856 | tf_op jit(solution)/shard_map/dot_general | solution.py:102
  145.8 0.0 all-reduce.6.cloned.1.call-update
  145.8 0.0 reduce-scatter.19.cloned.1.call-start
  145.9 0.1 fusion.4
  146.0 11.7 %psum.29 = bf16[32]{0:T(256)(128)(2,1)S(1)} all-reduce(bf16[32]{0:T(256)(128)(2,1)S(1)} %fusion.4), channel_id=1, replica_groups=mesh['grp'=2,'kv'=4,'tp'=4] {'kv'}, use_global_device_ids=true, to_apply=%region_11.12 | all-reduce | flops 32 | bytes 128 | tf_op jit(solution)/shard_map/psum | solution.py:107
  157.7 24.9 %all-reduce.6.cloned.1.call-done = (bf16[32,2752]{1,0:T(8,128)(2,1)}, bf16[32,2752]{1,0:T(8,128)(2,1)}) async-done(((bf16[32,2752]{1,0:T(8,128)(2,1)}, bf16[32,2752]{1,0:T(8,128)(2,1)}), (bf16[32,2752]{1,0:T(8,128)(2,1)}, bf16[32,2752]{1,0:T(8,128)(2,1)})) %all-reduce.6.cloned.1.call-update) | async-done | bytes 352272 | tf_op jit(solution)/shard_map/psum | solution.py:106
  182.6 4.6 %convolution_convert_fusion.2 = bf16[32,1024]{1,0:T(8,128)(2,1)} fusion(bf16[2752,1024]{1,0:T(8,128)(2,1)} %param.37, bf16[32,2752]{1,0:T(8,128)(2,1)} %get-tuple-element.11, bf16[32,2752]{1,0:T(8,128)(2,1)} %get-tuple-element.12, f32[32]{0:T(128)S(1)} %add_rsqrt_fusion), kind=kOutput, calls=%fused_computation.2 | convolution fusion | flops 181268480 | bytes 6054016 | tf_op jit(solution)/shard_map/dot_general | solution.py:111
  187.2 0.0 reduce-scatter.19.cloned.1.call-update
  187.2 0.7 copy.32
  187.9 18.9 %reduce-scatter.19.cloned.1.call-done = bf16[32,256]{1,0:T(8,128)(2,1)} async-done(((bf16[32,1024]{1,0:T(8,128)(2,1)}), bf16[32,256]{1,0:T(8,128)(2,1)}) %reduce-scatter.19.cloned.1.call-update) | async-done | bytes 16400 | tf_op jit(solution)/shard_map/reduce_scatter | solution.py:112
  206.7 1.3 add_convert_fusion
  (9 shorter events, 0.0 us)
Async XLA Ops:
  7.2 103.8 %copy-start = (bf16[512,1024]{1,0:T(8,128)(2,1)S(1)}, bf16[512,1024]{1,0:T(8,128)(2,1)}, u32[]{:S(2)}) copy-start(bf16[512,1024]{1,0:T(8,128)(2,1)} %param.33) | copy-start | bytes 3145732
  7.2 122.6 %copy-start.2 = (bf16[32,256]{1,0:T(8,128)(2,1)S(1)}, bf16[32,256]{1,0:T(8,128)(2,1)}, u32[]{:S(2)}) copy-start(bf16[32,256]{1,0:T(8,128)(2,1)} %param.19) | copy-start | bytes 49156
  7.2 104.7 %copy-start.3 = (bf16[1024]{0:T(1024)(128)(2,1)S(1)}, bf16[1024]{0:T(1024)(128)(2,1)}, u32[]{:S(2)}) copy-start(bf16[1024]{0:T(1024)(128)(2,1)} %param.34) | copy-start | bytes 6148
  7.2 35.0 %reduce-scatter.11.cloned.1.call-start = ((), (), s32[]{:S(2)}) async-start(), calls=%async_computation.7 | async-start | bytes 40960 | tf_op jit(solution)/shard_map/reduce_scatter | solution.py:70
  16.3 40.8 %reduce-scatter.9.cloned.1.call-start = ((), (), s32[]{:S(2)}) async-start(), calls=%async_computation.6 | async-start | bytes 40960 | tf_op jit(solution)/shard_map/reduce_scatter | solution.py:69
  18.2 59.2 %reduce-scatter.13.cloned.1.call-start = ((), (), s32[]{:S(2)}) async-start(), calls=%async_computation.8 | async-start | bytes 81920 | tf_op jit(solution)/shard_map/reduce_scatter | solution.py:71
  20.4 76.5 %reduce-scatter.15.cloned.1.call-start = ((), (), s32[]{:S(2)}) async-start(), calls=%async_computation.9 | async-start | bytes 81920 | tf_op jit(solution)/shard_map/reduce_scatter | solution.py:72
  22.6 107.1 %reduce-scatter.17.cloned.1.call-start = ((), (), s32[]{:S(2)}) async-start(), calls=%async_computation.10 | async-start | bytes 81920 | tf_op jit(solution)/shard_map/reduce_scatter | solution.py:94
  79.8 66.0 %copy-start.1 = (f32[8,4,64,128]{3,2,1,0:T(8,128)}, f32[8,4,64,128]{3,2,1,0:T(8,128)S(1)}, u32[]{:S(2)}) copy-start(f32[8,4,64,128]{3,2,1,0:T(8,128)S(1)} %multiply_add_fusion) | copy-start | bytes 3145732
  111.9 70.8 %all-reduce.6.cloned.1.call-start = ((), (), s32[]{:S(2)}) async-start(), calls=%async_computation.12 | async-start | bytes 720896 | tf_op jit(solution)/shard_map/psum | solution.py:106
  145.8 60.9 %reduce-scatter.19.cloned.1.call-start = ((), (), s32[]{:S(2)}) async-start(), calls=%async_computation.11 | async-start | bytes 81920 | tf_op jit(solution)/shard_map/reduce_scatter | solution.py:112
Sparse Core Ops, SparseCore 0:
  16.4 20.8 reduce-scatter.10
  39.6 17.4 reduce-scatter.8
  59.9 17.4 reduce-scatter.12
  79.5 17.4 reduce-scatter.14
  112.0 17.7 reduce-scatter.16
  145.9 36.6 all-reduce.5
  187.4 19.3 reduce-scatter.18
where the time goes:
time: 216 us; the launch traced here: 215 us
  waiting for transfers between devices  111 us (51%)
  blocking collectives  49.1 us (23%)
  matrix products  26.1 us (12%)
  between operations  14.9 us (7%)
  other arithmetic  10.7 us (5%)
  local copies, waits for them, and re-layouts  3.25 us (2%)
    psum x1, waiting for transfers between devices, body(): lax.psum(up_part.astype(jnp.bfloat16), 'kv').astype(jnp.float32)  24.9 us
    reduce_scatter x1, waiting for transfers between devices, body(): lax.psum_scatter(down_part.astype(jnp.bfloat16), 'tp', scatter_dimension=...  18.9 us
    reduce_scatter x1, waiting for transfers between devices, body(): lax.psum_scatter(attn_part.astype(jnp.bfloat16), 'tp', scatter_dimension=...  17.8 us
    reduce_scatter x1, waiting for transfers between devices, body(): lax.psum_scatter(part_value, 'kv', scatter_dimension=0, tiled=True)  17.8 us
    reduce_scatter x1, waiting for transfers between devices, body(): lax.psum_scatter(part_ogate, 'kv', scatter_dimension=0, tiled=True)  16.2 us
    reduce_scatter x1, waiting for transfers between devices, body(): lax.psum_scatter(part_query, 'kv', scatter_dimension=0, tiled=True)  14.9 us
    all_gather x1, blocking collectives, body(): lax.all_gather(merged, 'kv', axis=0, tiled=True)  13.1 us
    psum x1, blocking collectives, body(): all_squares = lax.psum(squares, 'kv')  12.6 us
  transfers between devices with their start and end apart: 7, of which 6 were waited for; matrix products, arithmetic and copies ran while one was open for 9% of the time, Pallas kernels for 0%

commit v1 on v0

--- a/solution.py
+++ b/solution.py
@@ -1,15 +1,386 @@
+import functools
+
 import jax
 import jax.numpy as jnp
 from jax import lax
+from jax.experimental import pallas as pl
+from jax.experimental.pallas import tpu as pltpu
 from jax.sharding import PartitionSpec as P
 
-D = 4096
-DK = 64
-DV = 128
-
-
-norm_eps = 1e-06
-igate_cap = 1.5
+F32 = jnp.float32
+BF16 = jnp.bfloat16
+MESH = pl.DeviceIdType.MESH
+NORM_EPS = 1e-06
+IGATE_CAP = 1.5
+LANES = 128
+CHUNK = 768
+
+
+def cuts(total):
+    out = []
+    for off in range(0, total, CHUNK):
+        width = min(CHUNK, total - off)
+        out.append((off, width, -(-width // LANES) * LANES))
+    return out
+
+
+def kernel(
+    nkv, ntp, d_model,
+    tokens, norm_gain, w_query, w_key, w_value, w_ogate, w_if_i, w_if_f, ib, fb,
+    state_c, state_n, state_m, head_gain, w_out, ffn_gain, w_gate, w_up, w_down,
+    out_tokens, out_c, out_n, out_m,
+    wp, wout, wg, wu, wd, sc, nc,
+    tok_all, normed, pj_send, pj_recv, ax_send, ax_recv, num, mg_send, mg_all,
+    at_send, at_recv, mid_own, mid_all, sq_send, sq_recv, gu_send, gu_recv, hid_send, hid_all,
+    dn_send, dn_recv,
+    wsem, osem,
+    tok_s, tok_r, pj_s, pj_r, ax_s, ax_r, mg_s, mg_r, at_s, at_r, mid_s, mid_r,
+    sq_s, sq_r, gu_s, gu_r, hid_s, hid_r, dn_s, dn_r,
+):
+    kv = lax.axis_index("kv")
+    tp = lax.axis_index("tp")
+    kv_peer = [lax.rem(kv + d, nkv) for d in range(1, nkv)]
+    tp_peer = [lax.rem(tp + d, ntp) for d in range(1, ntp)]
+    kv_src = [lax.rem(kv + nkv - d, nkv) for d in range(1, nkv)]
+    tp_src = [lax.rem(tp + ntp - d, ntp) for d in range(1, ntp)]
+    seqs = tokens.shape[0]
+    rows = seqs // nkv
+    tcols = tokens.shape[1]
+    heads, dk, dv = state_c.shape[1:]
+    qk = w_query.shape[1]
+    vv = w_value.shape[1]
+    half = qk + vv
+    ff = w_gate.shape[0]
+    chunks = cuts(ff)
+
+    def fetch(i, src, dst):
+        c = pltpu.make_async_copy(src, dst, wsem.at[i])
+        c.start()
+        return c
+
+    first = [
+        fetch(0, w_query, wp.at[:, pl.ds(0, qk)]),
+        fetch(1, w_key, wp.at[:, pl.ds(qk, qk)]),
+        fetch(2, w_value, wp.at[:, pl.ds(2 * qk, vv)]),
+        fetch(3, w_ogate, wp.at[:, pl.ds(2 * qk + vv, vv)]),
+    ]
+
+    barrier = pltpu.get_barrier_semaphore()
+    for p in kv_peer:
+        pl.semaphore_signal(barrier, inc=1, device_id={"kv": p}, device_id_type=MESH)
+    for p in tp_peer:
+        pl.semaphore_signal(barrier, inc=1, device_id={"tp": p}, device_id_type=MESH)
+    pl.semaphore_wait(barrier, nkv - 1 + ntp - 1)
+
+    def send(src, dst, ssem, rsem, dev):
+        c = pltpu.make_async_remote_copy(
+            src_ref=src, dst_ref=dst, send_sem=ssem, recv_sem=rsem,
+            device_id=dev, device_id_type=MESH,
+        )
+        c.start()
+        return c
+
+    pending = []
+
+    copies = [
+        send(tokens, tok_all.at[tp], tok_s.at[d], tok_r.at[d], {"tp": p})
+        for d, p in enumerate(tp_peer)
+    ]
+    pending += copies
+    tok_all[tp] = tokens[...]
+    for c in copies:
+        c.wait_recv()
+    sq = jnp.zeros((seqs, 1), F32)
+    for j in range(ntp):
+        t = tok_all[j].astype(F32)
+        sl = slice(j * tcols, (j + 1) * tcols)
+        normed[:, sl] = (t * norm_gain[:, sl].astype(F32)).astype(BF16)
+        sq = sq + jnp.sum(t * t, axis=1, keepdims=True)
+    x = normed[...]
+    nt = (((1,), (1,)), ((), ()))
+    gi = lax.dot_general(x, w_if_i[...], nt, preferred_element_type=F32)
+    gf = lax.dot_general(x, w_if_f[...], nt, preferred_element_type=F32)
+    lane = lax.broadcasted_iota(jnp.int32, (seqs, LANES), 1)
+    aux = jnp.where(lane == 2 * heads, sq, 0.0)
+    for h in range(heads):
+        aux = jnp.where(lane == h, gi[:, h : h + 1], aux)
+        aux = jnp.where(lane == heads + h, gf[:, h : h + 1], aux)
+    for k in range(nkv):
+        ax_send[k] = aux[k * rows : (k + 1) * rows]
+    copies = [
+        send(ax_send.at[p], ax_recv.at[kv], ax_s.at[d], ax_r.at[d], {"kv": p})
+        for d, p in enumerate(kv_peer)
+    ]
+    pending += copies
+    ax_copies = copies
+
+    for c in first:
+        c.wait()
+    late = [
+        fetch(4, state_c, sc),
+        fetch(5, w_out, wout),
+        fetch(6, w_gate, wg),
+        fetch(7, w_up, wu),
+        fetch(8, w_down, wd),
+    ]
+    lo = jnp.dot(x, wp[:, :half], preferred_element_type=F32)
+    hi = jnp.dot(x, wp[:, half:], preferred_element_type=F32)
+    for k in range(nkv):
+        r = slice(k * rows, (k + 1) * rows)
+        pj_send[k] = jnp.concatenate([lo[r], hi[r]], axis=0).astype(BF16)
+    copies = [
+        send(pj_send.at[p], pj_recv.at[kv], pj_s.at[d], pj_r.at[d], {"kv": p})
+        for d, p in enumerate(kv_peer)
+    ]
+    pending += copies
+
+    a = ax_send[kv]
+    for d, c in enumerate(ax_copies):
+        c.wait_recv()
+        a = a + ax_recv[kv_src[d]]
+    row_scale = lax.rsqrt(a[:, 2 * heads : 2 * heads + 1] / d_model + NORM_EPS)
+    igate = IGATE_CAP * jnp.tanh((row_scale * a[:, :heads] + ib[...]) / IGATE_CAP)
+    fgate = row_scale * a[:, heads : 2 * heads] + fb[...]
+    log_sig = jnp.minimum(fgate, 0.0) - jnp.log1p(jnp.exp(-jnp.abs(fgate)))
+    carried = log_sig + state_m[...].T
+    new_m = jnp.maximum(carried, igate)
+    keep = jnp.exp(carried - new_m)
+    write = jnp.exp(igate - new_m)
+    floor = jnp.exp(-new_m)
+    out_m[...] = new_m.T
+    late[0].wait()
+
+    s = pj_send[kv].astype(F32)
+    for d, c in enumerate(copies):
+        c.wait_recv()
+        s = s + pj_recv[kv_src[d]].astype(F32)
+
+    def piece(off, width):
+        top = off // half
+        return s[top * rows : (top + 1) * rows, off - top * half : off - top * half + width]
+
+    q = row_scale * piece(0, qk)
+    klane = lax.broadcasted_iota(jnp.int32, (rows, qk), 1) // dk
+    spread = jnp.zeros((rows, qk), F32)
+    for h in range(heads):
+        spread = jnp.where(klane == h, write[:, h : h + 1], spread)
+    kw = spread * (row_scale * piece(qk, qk) * dk ** (-0.5))
+    q_t = q.T
+    k_t = kw.T
+    for h in range(heads):
+        hk = slice(h * dk, (h + 1) * dk)
+        hv = slice(h * dv, (h + 1) * dv)
+        keep_h = jnp.broadcast_to(keep[:, h : h + 1], (rows, dv))
+        val = row_scale * piece(2 * qk + h * dv, dv)
+        for b in range(rows):
+            c_new = keep_h[b : b + 1] * sc[b, h] + k_t[hk, b : b + 1] * val[b : b + 1]
+            nc[b, h] = c_new
+            num[b : b + 1, hv] = jnp.sum(q_t[hk, b : b + 1] * c_new, axis=0, keepdims=True)
+        n_new = keep[:, h : h + 1] * state_n[:, h, :] + kw[:, hk]
+        out_n[:, h, :] = n_new
+        den = jnp.sum(q[:, hk] * n_new, axis=1, keepdims=True)
+        head_out = num[:, hv] / jnp.maximum(jnp.abs(den), floor[:, h : h + 1])
+        og = row_scale * piece(2 * qk + vv + h * dv, dv)
+        gated = head_out * head_gain[h : h + 1].astype(F32) * jax.nn.sigmoid(og)
+        mg_send[:, hv] = gated.astype(BF16)
+    copies = [
+        send(mg_send, mg_all.at[kv], mg_s.at[d], mg_r.at[d], {"kv": p})
+        for d, p in enumerate(kv_peer)
+    ]
+    pending += copies
+    c_out = pltpu.make_async_copy(nc, out_c, osem)
+    c_out.start()
+    mg_all[kv] = mg_send[...]
+    late[1].wait()
+    for c in copies:
+        c.wait_recv()
+    merged = jnp.concatenate([mg_all[k].astype(F32) for k in range(nkv)], axis=0).astype(BF16)
+
+    attn = jnp.dot(merged, wout[...], preferred_element_type=F32)
+    for j in range(ntp):
+        at_send[j] = attn[:, j * tcols : (j + 1) * tcols].astype(BF16)
+    copies = [
+        send(at_send.at[p], at_recv.at[tp], at_s.at[d], at_r.at[d], {"tp": p})
+        for d, p in enumerate(tp_peer)
+    ]
+    pending += copies
+    tot = at_send[tp].astype(F32)
+    for d, c in enumerate(copies):
+        c.wait_recv()
+        tot = tot + at_recv[tp_src[d]].astype(F32)
+    mid_own[...] = (tokens[...].astype(F32) + tot).astype(BF16)
+    copies = [
+        send(mid_own, mid_all.at[tp], mid_s.at[d], mid_r.at[d], {"tp": p})
+        for d, p in enumerate(tp_peer)
+    ]
+    pending += copies
+    mid_all[tp] = mid_own[...]
+    if chunks[-1][1] != chunks[-1][2]:
+        pad = chunks[-1][2] - chunks[-1][1]
+        gu_send[:, :, ff:] = jnp.zeros((nkv, 2 * rows, pad), BF16)
+        hid_send[:, ff:] = jnp.zeros((rows, pad), BF16)
+    late[2].wait()
+    late[3].wait()
+    for c in copies:
+        c.wait_recv()
+    sq = jnp.zeros((seqs, 1), F32)
+    for j in range(ntp):
+        t = mid_all[j].astype(F32)
+        sl = slice(j * tcols, (j + 1) * tcols)
+        normed[:, sl] = (t * ffn_gain[:, sl].astype(F32)).astype(BF16)
+        sq = sq + jnp.sum(t * t, axis=1, keepdims=True)
+    sq = jnp.broadcast_to(sq, (seqs, LANES))
+    for k in range(nkv):
+        sq_send[k] = sq[k * rows : (k + 1) * rows]
+    sq_copies = [
+        send(sq_send.at[p], sq_recv.at[kv], sq_s.at[d], sq_r.at[d], {"kv": p})
+        for d, p in enumerate(kv_peer)
+    ]
+    pending += sq_copies
+
+    x = normed[...]
+    gu_copies = []
+    for i, (off, width, wide) in enumerate(chunks):
+        g = lax.dot_general(x, wg[off : off + width], nt, preferred_element_type=F32)
+        u = lax.dot_general(x, wu[off : off + width], nt, preferred_element_type=F32)
+        for k in range(nkv):
+            r = slice(k * rows, (k + 1) * rows)
+            gu_send[k, :, off : off + width] = jnp.concatenate([g[r], u[r]], axis=0).astype(BF16)
+        window = pl.ds(off, wide)
+        copies = [
+            send(gu_send.at[p, :, window], gu_recv.at[kv, :, window],
+                 gu_s.at[i, d], gu_r.at[i, d], {"kv": p})
+            for d, p in enumerate(kv_peer)
+        ]
+        gu_copies.append(copies)
+        pending += copies
+
+    a = sq_send[kv]
+    for d, c in enumerate(sq_copies):
+        c.wait_recv()
+        a = a + sq_recv[kv_src[d]]
+    ffn_scale = lax.rsqrt(a[:, :1] / d_model + NORM_EPS)
+    hid_copies = []
+    for i, (off, width, wide) in enumerate(chunks):
+        t = gu_send[kv, :, off : off + wide].astype(F32)
+        for d, c in enumerate(gu_copies[i]):
+            c.wait_recv()
+            t = t + gu_recv[kv_src[d], :, off : off + wide].astype(F32)
+        g = ffn_scale * t[:rows]
+        hid = g / (1.0 + jnp.exp(-g)) * (ffn_scale * t[rows:])
+        hid_send[:, off : off + wide] = hid.astype(BF16)
+        window = pl.ds(off, wide)
+        copies = [
+            send(hid_send.at[:, window], hid_all.at[kv, :, window],
+                 hid_s.at[i, d], hid_r.at[i, d], {"kv": p})
+            for d, p in enumerate(kv_peer)
+        ]
+        hid_copies.append(copies)
+        pending += copies
+    hid_all[kv] = hid_send[...]
+    late[4].wait()
+    down = None
+    for i, (off, width, wide) in enumerate(chunks):
+        for c in hid_copies[i]:
+            c.wait_recv()
+        h = jnp.concatenate(
+            [hid_all[k, :, off : off + width].astype(F32) for k in range(nkv)], axis=0
+        ).astype(BF16)
+        part = jnp.dot(h, wd[off : off + width, :], preferred_element_type=F32)
+        down = part if down is None else down + part
+    for j in range(ntp):
+        dn_send[j] = down[:, j * tcols : (j + 1) * tcols].astype(BF16)
+    copies = [
+        send(dn_send.at[p], dn_recv.at[tp], dn_s.at[d], dn_r.at[d], {"tp": p})
+        for d, p in enumerate(tp_peer)
+    ]
+    pending += copies
+    tot = dn_send[tp].astype(F32)
+    for d, c in enumerate(copies):
+        c.wait_recv()
+        tot = tot + dn_recv[tp_src[d]].astype(F32)
+    out_tokens[...] = (mid_own[...].astype(F32) + tot).astype(BF16)
+    for c in pending:
+        c.wait_send()
+    c_out.wait()
+
+
+def layer(
+    nkv, ntp, d_model,
+    tokens, norm_gain, w_query, w_key, w_value, w_ogate, w_igate, w_fgate,
+    igate_bias, fgate_bias, state_c, state_n, state_m, head_gain,
+    w_out, ffn_gain, w_gate, w_up, w_down,
+):
+    seqs, tcols = tokens.shape
+    rows = seqs // nkv
+    depth, qk = w_query.shape
+    vv = w_value.shape[1]
+    half = qk + vv
+    ff = w_gate.shape[1]
+    nch = len(cuts(ff))
+    wide = -(-ff // LANES) * LANES
+    hbm = pl.BlockSpec(memory_space=pl.ANY)
+    vmem = pl.BlockSpec(memory_space=pltpu.VMEM)
+    dma = lambda *n: pltpu.SemaphoreType.DMA(n)
+    k, t = nkv - 1, ntp - 1
+    scratch = [
+        pltpu.VMEM((depth, 2 * half), BF16),
+        pltpu.VMEM(w_out.shape, BF16),
+        pltpu.VMEM(w_gate.shape[::-1], BF16),
+        pltpu.VMEM(w_up.shape[::-1], BF16),
+        pltpu.VMEM(w_down.shape, BF16),
+        pltpu.VMEM(state_c.shape, F32),
+        pltpu.VMEM(state_c.shape, F32),
+        pltpu.VMEM((ntp, seqs, tcols), BF16),
+        pltpu.VMEM((seqs, depth), BF16),
+        pltpu.VMEM((nkv, 2 * rows, half), BF16),
+        pltpu.VMEM((nkv, 2 * rows, half), BF16),
+        pltpu.VMEM((nkv, rows, LANES), F32),
+        pltpu.VMEM((nkv, rows, LANES), F32),
+        pltpu.VMEM((rows, vv), F32),
+        pltpu.VMEM((rows, vv), BF16),
+        pltpu.VMEM((nkv, rows, vv), BF16),
+        pltpu.VMEM((ntp, seqs, tcols), BF16),
+        pltpu.VMEM((ntp, seqs, tcols), BF16),
+        pltpu.VMEM((seqs, tcols), BF16),
+        pltpu.VMEM((ntp, seqs, tcols), BF16),
+        pltpu.VMEM((nkv, rows, LANES), F32),
+        pltpu.VMEM((nkv, rows, LANES), F32),
+        pltpu.VMEM((nkv, 2 * rows, wide), BF16),
+        pltpu.VMEM((nkv, 2 * rows, wide), BF16),
+        pltpu.VMEM((rows, wide), BF16),
+        pltpu.VMEM((nkv, rows, wide), BF16),
+        pltpu.VMEM((ntp, seqs, tcols), BF16),
+        pltpu.VMEM((ntp, seqs, tcols), BF16),
+        dma(9),
+        pltpu.SemaphoreType.DMA,
+        dma(t), dma(t), dma(k), dma(k), dma(k), dma(k), dma(k), dma(k), dma(t), dma(t), dma(t), dma(t),
+        dma(k), dma(k), dma(nch, k), dma(nch, k), dma(nch, k), dma(nch, k), dma(t), dma(t),
+    ]
+    in_specs = [
+        vmem, vmem, hbm, hbm, hbm, hbm, vmem, vmem, vmem, vmem,
+        hbm, vmem, vmem, vmem, hbm, vmem, hbm, hbm, hbm,
+    ]
+    out = pl.pallas_call(
+        functools.partial(kernel, nkv, ntp, d_model),
+        out_shape=(
+            jax.ShapeDtypeStruct(tokens.shape, BF16),
+            jax.ShapeDtypeStruct(state_c.shape, F32),
+            jax.ShapeDtypeStruct(state_n.shape, F32),
+            jax.ShapeDtypeStruct(state_m.shape[::-1], F32),
+        ),
+        in_specs=in_specs,
+        out_specs=(vmem, hbm, vmem, vmem),
+        scratch_shapes=scratch,
+        compiler_params=pltpu.CompilerParams(
+            collective_id=0, has_side_effects=True, vmem_limit_bytes=60 * 1024 * 1024
+        ),
+    )(
+        tokens, norm_gain[None], w_query, w_key, w_value, w_ogate, w_igate.T, w_fgate.T,
+        igate_bias[None], fgate_bias[None], state_c, state_n, state_m.T, head_gain,
+        w_out, ffn_gain[None], w_gate.T, w_up.T, w_down,
+    )
+    return (*out[:3], out[3].T)
 
 
 def cell_update(query, key_vec, value_vec, igate, fgate, state_c, state_n, state_m):
@@ -28,7 +399,7 @@
     return (new_c, new_n, new_m, head_out)
 
 
-def body(
+def plain_layer(
     tokens,
     norm_gain,
     w_query,
@@ -50,7 +421,8 @@
     w_down,
 ):
     seq_rows = state_c.shape[0]
-    heads_here = state_c.shape[1]
+    heads_here, DK, DV = state_c.shape[1:]
+    D = w_query.shape[0] * lax.axis_size("kv")
     token_cols = lax.all_gather(tokens, "tp", axis=1, tiled=True)
     token_vals = token_cols.astype(jnp.float32)
     normed = (token_vals * norm_gain.astype(jnp.float32)).astype(jnp.bfloat16)
@@ -73,12 +445,12 @@
         lax.psum_scatter(part_igate, "kv", scatter_dimension=0, tiled=True),
         lax.psum_scatter(part_fgate, "kv", scatter_dimension=0, tiled=True),
     )
-    row_scale = lax.rsqrt(sum_squares / D + norm_eps)[:, None]
+    row_scale = lax.rsqrt(sum_squares / D + NORM_EPS)[:, None]
     query = (row_scale * sum_query).reshape(seq_rows, heads_here, DK)
     key_vec = (row_scale * sum_key).reshape(seq_rows, heads_here, DK) * DK ** (-0.5)
     value_vec = (row_scale * sum_value).reshape(seq_rows, heads_here, DV)
     ogate = (row_scale * sum_ogate).reshape(seq_rows, heads_here, DV)
-    igate = igate_cap * jnp.tanh((row_scale * sum_igate + igate_bias) / igate_cap)
+    igate = IGATE_CAP * jnp.tanh((row_scale * sum_igate + igate_bias) / IGATE_CAP)
     fgate = row_scale * sum_fgate + fgate_bias
     new_c, new_n, new_m, head_out = cell_update(
         query, key_vec, value_vec, igate, fgate, state_c, state_n, state_m
@@ -106,7 +478,7 @@
         lax.psum(up_part.astype(jnp.bfloat16), "kv").astype(jnp.float32),
         lax.psum(squares_two.astype(jnp.bfloat16), "kv").astype(jnp.float32),
     )
-    ffn_scale = lax.rsqrt(total_two / D + norm_eps)[:, None]
+    ffn_scale = lax.rsqrt(total_two / D + NORM_EPS)[:, None]
     hidden = (jax.nn.silu(ffn_scale * gate_sum) * (ffn_scale * up_sum)).astype(jnp.bfloat16)
     down_part = jnp.dot(hidden, w_down, preferred_element_type=jnp.float32)
     down_out = lax.psum_scatter(
@@ -117,6 +489,7 @@
 
 
 def solution(mesh):
+    nkv, ntp = mesh.shape["kv"], mesh.shape["tp"]
     placed = (
         P("grp", ("kv", "tp")),
         P("kv"),
@@ -138,6 +511,16 @@
         P("kv", "tp"),
         P("tp", "kv"),
     )
+
+    def body(*args):
+        d_model = args[2].shape[0] * nkv
+        seqs, tcols = args[0].shape
+        qk, vv = args[2].shape[1], args[4].shape[1]
+        whole_tiles = tcols % LANES == 0 and qk % LANES == 0 and vv % LANES == 0
+        if not whole_tiles or (seqs // nkv) % 8:
+            return plain_layer(*args)
+        return layer(nkv, ntp, d_model, *args)
+
     return jax.shard_map(
         body,
         mesh=mesh,

time: 216 us -> 54.9 us (0.25)
  waiting for transfers between devices: 111 us -> 0 us
  blocking collectives: 49.1 us -> 0 us
  Pallas kernels: 0 us -> 45 us
  matrix products: 26.1 us -> 0 us
  between operations: 14.9 us -> 0.64 us
  other arithmetic: 10.7 us -> 0 us
  local copies, waits for them, and re-layouts: 3.25 us -> 8.75 us
    reduce_scatter x6 -> x0, waiting for transfers between devices: 85.5 us -> none  [the longest x1 18.9 us: body(): lax.psum_scatter(down_part.astype(jnp.bfloat16), 'tp', scatter_dimension=...]
    pallas_call x0 -> x1, Pallas kernels: none -> 45 us  [layer(): pl.pallas_call(functools.partial(kernel, nkv, ntp, d_model), out_shape=(j...]
    dot_general x11 -> x0, matrix products: 26.1 us -> none  [the longest x1 5.03 us: body(): gate_part = jnp.dot(normed_two, w_gate, preferred_element_type=jnp.float32)]
    psum x1 -> x0, waiting for transfers between devices: 24.9 us -> none  [body(): lax.psum(up_part.astype(jnp.bfloat16), 'kv').astype(jnp.float32)]
    all_gather x3 -> x0, blocking collectives: 24.8 us -> none  [the longest x1 13.1 us: body(): lax.all_gather(merged, 'kv', axis=0, tiled=True)]
    psum x2 -> x0, blocking collectives: 24.3 us -> none  [the longest x1 12.6 us: body(): all_squares = lax.psum(squares, 'kv')]
    convert_element_type x6 -> x0, other arithmetic: 4.3 us -> none  [the longest x1 1.33 us: body(): out_tokens = (middle.astype(jnp.float32) + down_out).astype(jnp.bfloat16)]
    unnamed x12 -> x4, local copies, waits for them, and re-layouts: 2.75 us -> 6.2 us
  transfers between devices with their start and end apart: 7 -> 0, of which waited for: 6 -> 0; matrix products, arithmetic and copies ran while one was open for 9% -> 0% of each run, Pallas kernels for 0% -> 0%
where the time goes in v1:
time: 54.9 us; the launch traced here: 54.4 us
  Pallas kernels  45 us (82%)
  local copies, waits for them, and re-layouts  8.75 us (16%)
  between operations  0.64 us (1%)
    pallas_call x1, Pallas kernels, layer(): pl.pallas_call(functools.partial(kernel, nkv, ntp, d_model), out_shape=(j...  45 us
    unnamed x4, local copies, waits for them, and re-layouts  6.2 us
    broadcast_in_dim x1, local copies, waits for them, and re-layouts, layer(): norm_gain[None]  1.28 us
    broadcast_in_dim x1, local copies, waits for them, and re-layouts, layer(): ffn_gain[None]  1.28 us

profile of v1, /device:TPU:0, one launch (start us, length us, event | category | flops | bytes accessed | tf_op | source)
XLA Modules:
  0.0 54.4 jit_solution(1746752446796450063)
XLA Ops:
  0.6 1.3 %broadcast_in_dim.12.norm_gain = bf16[1,1024]{1,0:T(2,128)(2,1)} reshape(bf16[1024]{0:T(1024)(128)(2,1)} %param.20) | data formatting | bytes 4096 | tf_op jit(solution)/shard_map/broadcast_in_dim | solution.py:379
  1.9 1.3 %broadcast_in_dim.15.ffn_gain = bf16[1,1024]{1,0:T(2,128)(2,1)} reshape(bf16[1024]{0:T(1024)(128)(2,1)} %param.34) | data formatting | bytes 4096 | tf_op jit(solution)/shard_map/broadcast_in_dim | solution.py:381
  3.2 45.0 %shard_map.210 = (bf16[32,256]{1,0:T(8,128)(2,1)}, f32[8,4,64,128]{3,2,1,0:T(8,128)}, f32[8,4,64]{2,1,0:T(4,128)}, f32[4,8]{1,0:T(4,128)}) custom-call(bf16[32,256]{1,0:T(8,128)(2,1)} %tokens.1, bf16[1,1024]{1,0:T(2,128)(2,1)} %broadcast_in_dim.12.norm_gain, bf16[1024,256]{1,0:T(8,128)(2,1)} %w_query.1, bf16[1024,256]{1,0:T(8,128)(2,1)} %w_key.1, ...), custom_call_target="tpu_custom_call" | custom-call | tf_op jit(solution)/shard_map/pallas_call | solution.py:364
  48.2 1.3 %copy.27 = bf16[32,256]{1,0:T(8,128)(2,1)} copy(bf16[32,256]{1,0:T(8,128)(2,1)} %get-tuple-element.16) | data formatting | bytes 32768
  49.5 2.3 %copy.28 = f32[8,4,64,128]{3,2,1,0:T(8,128)} copy(f32[8,4,64,128]{3,2,1,0:T(8,128)} %get-tuple-element.17) | data formatting | bytes 2097152
  51.8 1.3 %copy.29 = f32[8,4,64]{2,1,0:T(4,128)} copy(f32[8,4,64]{2,1,0:T(4,128)} %get-tuple-element.18) | data formatting | bytes 16384
  53.2 1.2 %copy.30 = f32[8,4]{0,1:T(4,128)} copy(f32[8,4]{0,1:T(4,128)} %bitcast.13) | data formatting | bytes 256

commit v2 on v1

--- a/solution.py
+++ b/solution.py
@@ -14,6 +14,7 @@
 IGATE_CAP = 1.5
 LANES = 128
 CHUNK = 768
+PARTS = 4
 
 
 def cuts(total):
@@ -26,14 +27,15 @@
 
 def kernel(
     nkv, ntp, d_model,
-    tokens, norm_gain, w_query, w_key, w_value, w_ogate, w_if_i, w_if_f, ib, fb,
-    state_c, state_n, state_m, head_gain, w_out, ffn_gain, w_gate, w_up, w_down,
+    tokens_in, norm_gain_in, w_query, w_key, w_value, w_ogate, w_if_i_in, w_if_f_in, ib_in, fb_in,
+    state_c, state_n_in, state_m_in, head_gain_in, w_out, ffn_gain_in, w_gate, w_up, w_down,
     out_tokens, out_c, out_n, out_m,
+    tokens, norm_gain, w_if_i, w_if_f, ib, fb, state_n, state_m, head_gain, ffn_gain,
     wp, wout, wg, wu, wd, sc, nc,
     tok_all, normed, pj_send, pj_recv, ax_send, ax_recv, num, mg_send, mg_all,
     at_send, at_recv, mid_own, mid_all, sq_send, sq_recv, gu_send, gu_recv, hid_send, hid_all,
     dn_send, dn_recv,
-    wsem, osem,
+    wsem, osem, small_sem,
     tok_s, tok_r, pj_s, pj_r, ax_s, ax_r, mg_s, mg_r, at_s, at_r, mid_s, mid_r,
     sq_s, sq_r, gu_s, gu_r, hid_s, hid_r, dn_s, dn_r,
 ):
@@ -53,11 +55,26 @@
     ff = w_gate.shape[0]
     chunks = cuts(ff)
 
+    barrier = pltpu.get_barrier_semaphore()
+    for p in kv_peer:
+        pl.semaphore_signal(barrier, inc=1, device_id={"kv": p}, device_id_type=MESH)
+    for p in tp_peer:
+        pl.semaphore_signal(barrier, inc=1, device_id={"tp": p}, device_id_type=MESH)
+
     def fetch(i, src, dst):
         c = pltpu.make_async_copy(src, dst, wsem.at[i])
         c.start()
         return c
 
+    small = []
+    for i, (src, dst) in enumerate([
+        (tokens_in, tokens), (norm_gain_in, norm_gain), (w_if_i_in, w_if_i), (w_if_f_in, w_if_f),
+        (ib_in, ib), (fb_in, fb), (state_n_in, state_n), (state_m_in, state_m),
+        (head_gain_in, head_gain), (ffn_gain_in, ffn_gain),
+    ]):
+        c = pltpu.make_async_copy(src, dst, small_sem.at[i])
+        c.start()
+        small.append(c)
     first = [
         fetch(0, w_query, wp.at[:, pl.ds(0, qk)]),
         fetch(1, w_key, wp.at[:, pl.ds(qk, qk)]),
@@ -65,11 +82,7 @@
         fetch(3, w_ogate, wp.at[:, pl.ds(2 * qk + vv, vv)]),
     ]
 
-    barrier = pltpu.get_barrier_semaphore()
-    for p in kv_peer:
-        pl.semaphore_signal(barrier, inc=1, device_id={"kv": p}, device_id_type=MESH)
-    for p in tp_peer:
-        pl.semaphore_signal(barrier, inc=1, device_id={"tp": p}, device_id_type=MESH)
+    small[0].wait()
     pl.semaphore_wait(barrier, nkv - 1 + ntp - 1)
 
     def send(src, dst, ssem, rsem, dev):
@@ -80,6 +93,12 @@
         c.start()
         return c
 
+    def scaled(t, j, gain):
+        for c in range(tcols // LANES):
+            g = j * (tcols // LANES) + c
+            part = t[:, c * LANES : (c + 1) * LANES] * gain[g : g + 1].astype(F32)
+            normed[:, g * LANES : (g + 1) * LANES] = part.astype(BF16)
+
     pending = []
 
     copies = [
@@ -88,13 +107,14 @@
     ]
     pending += copies
     tok_all[tp] = tokens[...]
+    for c in small[1:]:
+        c.wait()
     for c in copies:
         c.wait_recv()
     sq = jnp.zeros((seqs, 1), F32)
     for j in range(ntp):
         t = tok_all[j].astype(F32)
-        sl = slice(j * tcols, (j + 1) * tcols)
-        normed[:, sl] = (t * norm_gain[:, sl].astype(F32)).astype(BF16)
+        scaled(t, j, norm_gain)
         sq = sq + jnp.sum(t * t, axis=1, keepdims=True)
     x = normed[...]
     nt = (((1,), (1,)), ((), ()))
@@ -226,8 +246,7 @@
     sq = jnp.zeros((seqs, 1), F32)
     for j in range(ntp):
         t = mid_all[j].astype(F32)
-        sl = slice(j * tcols, (j + 1) * tcols)
-        normed[:, sl] = (t * ffn_gain[:, sl].astype(F32)).astype(BF16)
+        scaled(t, j, ffn_gain)
         sq = sq + jnp.sum(t * t, axis=1, keepdims=True)
     sq = jnp.broadcast_to(sq, (seqs, LANES))
     for k in range(nkv):
@@ -305,6 +324,24 @@
     c_out.wait()
 
 
+def hand_over(tok, c, n, m, tok_out, c_out, n_out, m_out, tok_v, c_v, n_v, m_v, isem, osem):
+    size = c.shape[0] // PARTS
+    moves = []
+    for i in range(PARTS):
+        window = pl.ds(i * size, size)
+        moves.append((c.at[window], c_v.at[window], c_out.at[window]))
+    moves += [(tok, tok_v, tok_out), (n, n_v, n_out), (m, m_v, m_out)]
+    into = [pltpu.make_async_copy(a, b, isem.at[i]) for i, (a, b, _) in enumerate(moves)]
+    out = [pltpu.make_async_copy(b, o, osem.at[i]) for i, (_, b, o) in enumerate(moves)]
+    for x in into:
+        x.start()
+    for x, y in zip(into, out):
+        x.wait()
+        y.start()
+    for y in out:
+        y.wait()
+
+
 def layer(
     nkv, ntp, d_model,
     tokens, norm_gain, w_query, w_key, w_value, w_ogate, w_igate, w_fgate,
@@ -323,7 +360,11 @@
     vmem = pl.BlockSpec(memory_space=pltpu.VMEM)
     dma = lambda *n: pltpu.SemaphoreType.DMA(n)
     k, t = nkv - 1, ntp - 1
-    scratch = [
+    smalls = (
+        tokens, norm_gain.reshape(-1, LANES), w_igate.T, w_fgate.T, igate_bias[None],
+        fgate_bias[None], state_n, state_m.T, head_gain, ffn_gain.reshape(-1, LANES),
+    )
+    scratch = [pltpu.VMEM(x.shape, x.dtype) for x in smalls] + [
         pltpu.VMEM((depth, 2 * half), BF16),
         pltpu.VMEM(w_out.shape, BF16),
         pltpu.VMEM(w_gate.shape[::-1], BF16),
@@ -354,12 +395,9 @@
         pltpu.VMEM((ntp, seqs, tcols), BF16),
         dma(9),
         pltpu.SemaphoreType.DMA,
+        dma(len(smalls)),
         dma(t), dma(t), dma(k), dma(k), dma(k), dma(k), dma(k), dma(k), dma(t), dma(t), dma(t), dma(t),
         dma(k), dma(k), dma(nch, k), dma(nch, k), dma(nch, k), dma(nch, k), dma(t), dma(t),
-    ]
-    in_specs = [
-        vmem, vmem, hbm, hbm, hbm, hbm, vmem, vmem, vmem, vmem,
-        hbm, vmem, vmem, vmem, hbm, vmem, hbm, hbm, hbm,
     ]
     out = pl.pallas_call(
         functools.partial(kernel, nkv, ntp, d_model),
@@ -369,18 +407,24 @@
             jax.ShapeDtypeStruct(state_n.shape, F32),
             jax.ShapeDtypeStruct(state_m.shape[::-1], F32),
         ),
-        in_specs=in_specs,
+        in_specs=[hbm] * 19,
         out_specs=(vmem, hbm, vmem, vmem),
         scratch_shapes=scratch,
         compiler_params=pltpu.CompilerParams(
             collective_id=0, has_side_effects=True, vmem_limit_bytes=60 * 1024 * 1024
         ),
     )(
-        tokens, norm_gain[None], w_query, w_key, w_value, w_ogate, w_igate.T, w_fgate.T,
-        igate_bias[None], fgate_bias[None], state_c, state_n, state_m.T, head_gain,
-        w_out, ffn_gain[None], w_gate.T, w_up.T, w_down,
-    )
-    return (*out[:3], out[3].T)
+        *smalls[:2], w_query, w_key, w_value, w_ogate, *smalls[2:6], state_c, *smalls[6:9],
+        w_out, smalls[9], w_gate.T, w_up.T, w_down,
+    )
+    tok, new_c, new_n, new_m = pl.pallas_call(
+        hand_over,
+        out_shape=tuple(jax.ShapeDtypeStruct(o.shape, o.dtype) for o in out),
+        in_specs=[hbm] * 4,
+        out_specs=(hbm,) * 4,
+        scratch_shapes=[pltpu.VMEM(o.shape, o.dtype) for o in out] + [dma(PARTS + 3), dma(PARTS + 3)],
+    )(*out)
+    return tok, new_c, new_n, new_m.T
 
 
 def cell_update(query, key_vec, value_vec, igate, fgate, state_c, state_n, state_m):

time: 54.9 us -> 47.3 us (0.86)
  local copies, waits for them, and re-layouts: 8.75 us -> 0 us
  Pallas kernels: 45 us -> 46.4 us
    unnamed x4 -> x0, local copies, waits for them, and re-layouts: 6.2 us -> none
    broadcast_in_dim x2 -> x0, local copies, waits for them, and re-layouts: 2.56 us -> none  [the longest x1 1.28 us: layer(): norm_gain[None]]
    pallas_call x0 -> x1, Pallas kernels: none -> 2.04 us  [layer(): pl.pallas_call(hand_over, out_shape=tuple((jax.ShapeDtypeStruct(o.shape,...]
    pallas_call x1, Pallas kernels: 45 us -> 44.4 us  [layer(): pl.pallas_call(functools.partial(kernel, nkv, ntp, d_model), out_shape=(j...]
where the time goes in v2:
time: 47.3 us; the launch traced here: 47 us
  Pallas kernels  46.4 us (98%)
  between operations  0.65 us (1%)
    pallas_call x1, Pallas kernels, layer(): pl.pallas_call(functools.partial(kernel, nkv, ntp, d_model), out_shape=(j...  44.4 us
    pallas_call x1, Pallas kernels, layer(): pl.pallas_call(hand_over, out_shape=tuple((jax.ShapeDtypeStruct(o.shape,...  2.04 us

profile of v2, /device:TPU:0, one launch (start us, length us, event | category | flops | bytes accessed | tf_op | source)
XLA Modules:
  0.0 47.0 jit_solution(17061066002834208864)
XLA Ops:
  0.6 44.4 %shard_map.210 = (bf16[32,256]{1,0:T(8,128)(2,1)}, f32[8,4,64,128]{3,2,1,0:T(8,128)}, f32[8,4,64]{2,1,0:T(4,128)}, f32[4,8]{1,0:T(4,128)}) custom-call(bf16[32,256]{1,0:T(8,128)(2,1)} %tokens_in.1, bf16[8,128]{1,0:T(8,128)(2,1)} %bitcast.14, bf16[1024,256]{1,0:T(8,128)(2,1)} %w_query.1, bf16[1024,256]{1,0:T(8,128)(2,1)} %w_key.1, bf16[1024,512]{1,0:T(8,128)(2,1)} %w_value.1, ...), custom_call_target="tpu_custom_call" | custom-call | tf_op jit(solution)/shard_map/pallas_call | solution.py:402
  45.0 2.0 %shard_map.211 = (bf16[32,256]{1,0:T(8,128)(2,1)}, f32[8,4,64,128]{3,2,1,0:T(8,128)}, f32[8,4,64]{2,1,0:T(4,128)}, f32[4,8]{1,0:T(4,128)}) custom-call(bf16[32,256]{1,0:T(8,128)(2,1)} %get-tuple-element.12.tok, f32[8,4,64,128]{3,2,1,0:T(8,128)} %get-tuple-element.13.c, f32[8,4,64]{2,1,0:T(4,128)} %get-tuple-element.14.n, f32[4,8]{1,0:T(4,128)} %get-tuple-element.15.m), custom_call_target="tpu_custom_call" | custom-call | tf_op jit(solution)/shard_map/pallas_call | solution.py:420
